TPU v7x, 512 devices: a whole 4x8x8 slice. The times are simulated.
512 devices in a mesh: sp: 64 (over z, y), tp: 8 (over x, core).
Axes of the slice: x: 4, y: 8, z: 8, core: 2. Of those that a mesh axis runs over, the one named last changes fastest.
Arguments:
- tokens: bfloat16 [16384, 1024], P(('sp', 'tp')), may hold values from -16 to 16, as said below
- valid_len: int32 [1], replicated, may hold values from 12288 to 16384
- norm_gain: float32 [1024], replicated, may hold values from 0.5 to 1.5
- w_query: bfloat16 [1024, 4096], P(None, 'tp'), may hold values from -0.1875 to 0.1875
- w_key: bfloat16 [1024, 1024], P(None, 'tp'), may hold values from -0.1875 to 0.1875
- w_value: bfloat16 [1024, 1024], P(None, 'tp'), may hold values from -0.1875 to 0.1875
- q_gain: float32 [128], replicated, may hold values from 0.5 to 1.5
- k_gain: float32 [128], replicated, may hold values from 0.5 to 1.5
- w_out: bfloat16 [4096, 1024], P('tp'), may hold values from -0.375 to 0.375
Outputs:
- mixed: bfloat16 [16384, 1024], P(('sp', 'tp'))
Inputs may be any that keep to these rules, and one draw needn't show every extreme that they name: tokens are random entries of unit-order spread (normal or uniform) plus a shift shared by every run of 256 consecutive rows, within -16 and 16. valid_len is at least three quarters of 16384 and at most 16384.
All inputs are finite; a program needn't handle non-finite values.
Results may differ from a plain program's by a relative error of at most 0.02.
Values may be sent and summed in bfloat16 or wider, within the bound.
A program may use at most 64 MiB of HBM per device.

v0:
```python
import functools
import math

import jax
import jax.numpy as jnp
from jax import lax
from jax.experimental import pallas as pl
from jax.experimental.pallas import tpu as pltpu
from jax.sharding import PartitionSpec as P

HEAD_DIM = 128
Q_PER_KV = 4
GRID_W = 64
CHUNK_BLOCKS = 2
FUSED = True

norm_eps = 1e-06
rope_base = 10000.0


def angle_tables(index, head_width, halves):
    quarter = head_width // 4
    frequency = rope_base ** (-(jnp.arange(quarter, dtype=jnp.float32) * 2.0) / (head_width // 2))
    angle = index.astype(jnp.float32)[:, None] * frequency[None, :]
    cosine, sine, zero = jnp.cos(angle), jnp.sin(angle), jnp.zeros_like(angle)
    blank = [zero, zero]

    def lay(pair):
        return jnp.concatenate(pair + blank if halves == 0 else blank + pair, axis=-1)

    return jnp.stack([lay([cosine, cosine]), lay([zero, sine]), lay([-sine, zero])])


def with_gain(tables, gain, factor):
    quarter = gain.shape[0] // 4
    gains = jnp.stack([gain, jnp.roll(gain, quarter), jnp.roll(gain, -quarter)])
    return tables * (gains * factor)[:, None, :]


def unit_rows(rows, gain):
    wide = rows.astype(jnp.float32)
    scale = lax.rsqrt(jnp.mean(wide * wide, axis=-1, keepdims=True) + norm_eps)
    return (wide * scale * gain).astype(jnp.bfloat16)


def rotate(part, tables):
    width = part.shape[-1]
    scale = lax.rsqrt(jnp.mean(part * part, axis=-1, keepdims=True) + norm_eps)
    ahead = pltpu.roll(part, width // 4, 1)
    behind = pltpu.roll(part, width - width // 4, 1)
    return (part * tables[0] + ahead * tables[1] + behind * tables[2]) * scale


def project_queries(own, gain_ref, w_query_ref, q_tab_ref, q_scr, block_rows):
    groups = q_scr.shape[0]
    normed = unit_rows(own, gain_ref[...])
    tables = [q_tab_ref[i] for i in range(3)]
    span = Q_PER_KV * HEAD_DIM
    for g in range(groups):
        projected = jnp.dot(
            normed, w_query_ref[:, g * span:(g + 1) * span], preferred_element_type=jnp.float32
        )
        for r in range(Q_PER_KV):
            head = rotate(projected[:, r * HEAD_DIM:(r + 1) * HEAD_DIM], tables)
            q_scr[g, r * block_rows:(r + 1) * block_rows, :] = head.astype(jnp.bfloat16)


def fold_chunk(start, chunk, tok_ref, valid_ref, gain_ref, w_key_ref, w_value_ref, row_tab_ref,
               col_tab_ref, q_scr, key_scr, val_scr, acc_scr, block_rows):
    groups = q_scr.shape[0]
    normed = unit_rows(tok_ref[pl.ds(start, chunk), :], gain_ref[...])
    keys = jnp.dot(normed, w_key_ref[...], preferred_element_type=jnp.float32)
    grid_rows = chunk // GRID_W
    first = pl.multiple_of(start // GRID_W, grid_rows)
    tables = []
    for i in range(3):
        rows = row_tab_ref[i, pl.ds(first, grid_rows), :]
        cols = col_tab_ref[i]
        tables.append(jnp.concatenate([rows[j:j + 1] + cols for j in range(grid_rows)], axis=0))
    for g in range(groups):
        turned = rotate(keys[:, g * HEAD_DIM:(g + 1) * HEAD_DIM], tables)
        key_scr[g] = turned.T.astype(jnp.bfloat16)
    values = jnp.dot(normed, w_value_ref[...], preferred_element_type=jnp.float32)
    at = start + lax.broadcasted_iota(jnp.int32, (chunk, HEAD_DIM), 0)
    kept = at < valid_ref[0]
    ones = jnp.where(kept, 1.0, 0.0).astype(jnp.bfloat16)
    for g in range(groups):
        part = values[:, g * HEAD_DIM:(g + 1) * HEAD_DIM]
        val_scr[g, :, :HEAD_DIM] = jnp.where(kept, part, 0.0).astype(jnp.bfloat16)
        val_scr[g, :, HEAD_DIM:] = ones

    def one_group(g, carry):
        for r in range(Q_PER_KV):
            span = slice(r * block_rows, (r + 1) * block_rows)
            scores = jnp.dot(q_scr[g, span, :], key_scr[g], preferred_element_type=jnp.float32)
            weights = jnp.exp2(scores).astype(jnp.bfloat16)
            acc_scr[g, span, :] += jnp.dot(
                weights, val_scr[g], preferred_element_type=jnp.float32
            )
        return carry

    lax.fori_loop(0, groups, one_group, 0)


def mix_heads(acc_scr, att_scr, block_rows):
    groups = acc_scr.shape[0]
    for g in range(groups):
        for r in range(Q_PER_KV):
            part = acc_scr[g, r * block_rows:(r + 1) * block_rows, :]
            head = g * Q_PER_KV + r
            att_scr[:, head * HEAD_DIM:(head + 1) * HEAD_DIM] = (
                part[:, :HEAD_DIM] / part[:, HEAD_DIM:]
            ).astype(jnp.bfloat16)


def local_kernel(block_rows, valid_ref, own_ref, tok_ref, gain_ref, w_query_ref, w_key_ref,
                 w_value_ref, w_out_ref, q_tab_ref, row_tab_ref, col_tab_ref, out_ref,
                 q_scr, key_scr, val_scr, acc_scr, att_scr):
    chunk = key_scr.shape[2]
    project_queries(own_ref[...], gain_ref, w_query_ref, q_tab_ref, q_scr, block_rows)
    acc_scr[...] = jnp.zeros_like(acc_scr)

    def step(i, carry):
        start = pl.multiple_of(i * chunk, chunk)
        fold_chunk(start, chunk, tok_ref, valid_ref, gain_ref, w_key_ref, w_value_ref,
                   row_tab_ref, col_tab_ref, q_scr, key_scr, val_scr, acc_scr, block_rows)
        return carry

    lax.fori_loop(0, tok_ref.shape[0] // chunk, step, 0)
    mix_heads(acc_scr, att_scr, block_rows)
    out_ref[...] = jnp.dot(
        att_scr[...], w_out_ref[...], preferred_element_type=jnp.float32
    ).astype(jnp.bfloat16)


def line_place(k, z, length):
    upper = (2 * z) // length
    near = z + upper * (length - 1 - 2 * z)
    far = (k + 1) // 2
    side = 2 * (k % 2) - 1
    beyond = jnp.minimum(k // (2 * near + 1), 1)
    mirrored = beyond * k + (1 - beyond) * (near + side * far)
    return mirrored + upper * (length - 1 - 2 * mirrored)


def fused_kernel(block_rows, total_sp, valid_ref, own_ref, gain_ref, w_query_ref, w_key_ref,
                 w_value_ref, w_out_ref, q_tab_ref, row_tab_ref, col_tab_ref, out_ref,
                 tok_ref, q_scr, key_scr, val_scr, acc_scr, att_scr, give_scr, take_scr,
                 col_recv, x_recv, y_recv, xd_recv, yd_recv, mate_recv,
                 up_send, down_send, x_send, y_send, xd_send, yd_send, mate_send, last_sem):
    chunk = key_scr.shape[2]
    half = block_rows // 2
    quart = half // 2
    length = total_sp // 4
    me = lax.axis_index("sp")
    core = lax.axis_index("tp")
    z, y, x = me // 4, (me // 2) % 2, me % 2
    x_mate = me + 1 - 2 * x
    y_mate = me + 2 - 4 * y
    d_mate = x_mate + 2 - 4 * y
    x_at, y_at, d_at = x_mate - 4 * z, y_mate - 4 * z, d_mate - 4 * z
    me_at = me - 4 * z

    def row_of(chip, which):
        return pl.multiple_of((chip * 2 + which) * half, half)

    def copy(row, count, device, send, recv, source=None):
        row = pl.multiple_of(row, count)
        here = tok_ref.at[pl.ds(row, count), :]
        return pltpu.make_async_remote_copy(
            src_ref=here if source is None else source,
            dst_ref=here,
            send_sem=send,
            recv_sem=recv,
            device_id=device,
            device_id_type=pl.DeviceIdType.MESH,
        )

    to_mate = {"sp": me, "tp": 1 - core}
    to_x = {"sp": x_mate, "tp": core}
    to_y = {"sp": y_mate, "tp": core}
    to_up = {"sp": me + 4, "tp": core}
    to_down = {"sp": me - 4, "tp": core}

    barrier = pltpu.get_barrier_semaphore()

    def greet(device):
        pl.semaphore_signal(barrier, inc=1, device_id=device, device_id_type=pl.DeviceIdType.MESH)

    greet(to_mate)
    greet(to_x)
    greet(to_y)

    @pl.when(z < length - 1)
    def _():
        greet(to_up)

    @pl.when(z > 0)
    def _():
        greet(to_down)

    has_up = jnp.minimum(length - 1 - z, 1)
    has_down = jnp.minimum(z, 1)
    pl.semaphore_wait(barrier, 3 + has_up + has_down)

    def mate_copy(chip, source=None):
        return copy(row_of(chip, core), half, to_mate, mate_send.at[chip], mate_recv.at[chip],
                    source)

    def mate_wait(chip):
        copy(row_of(chip, 1 - core), half, to_mate, mate_send.at[chip],
             mate_recv.at[chip]).wait_recv()

    def up_copy(layer, source=None):
        return copy(row_of(4 * layer + me_at, core), half, to_up, up_send.at[layer],
                    col_recv.at[layer], source)

    def down_copy(layer, source=None):
        return copy(row_of(4 * layer + me_at, core), half, to_down, down_send.at[layer],
                    col_recv.at[layer], source)

    def x_copy(layer, source=None):
        return copy(row_of(4 * layer + me_at, core), half, to_x, x_send.at[layer],
                    x_recv.at[layer], source)

    def y_copy(layer, source=None):
        return copy(row_of(4 * layer + me_at, core), half, to_y, y_send.at[layer],
                    y_recv.at[layer], source)

    def yd_copy(layer, at):
        return copy(row_of(4 * layer + at, core), quart, to_y, yd_send.at[layer],
                    yd_recv.at[layer])

    def xd_copy(layer, at):
        return copy(row_of(4 * layer + at, core) + quart, quart, to_x, xd_send.at[layer],
                    xd_recv.at[layer])

    def spread(layer, source=None):
        @pl.when(jnp.logical_and(layer <= z, z < length - 1))
        def _():
            up_copy(layer, source).start()

        @pl.when(jnp.logical_and(layer >= z, z > 0))
        def _():
            down_copy(layer, source).start()

        x_copy(layer, source).start()
        y_copy(layer, source).start()
        mate_copy(4 * layer + me_at, source).start()

    spread(z, own_ref)
    tok_ref[pl.ds(row_of(me, core), half), :] = own_ref[...]
    acc_scr[...] = jnp.zeros_like(acc_scr)
    mate_wait(me)
    project_queries(tok_ref[pl.ds(row_of(me, 0), block_rows), :], gain_ref, w_query_ref,
                    q_tab_ref, q_scr, block_rows)

    def fold(start):
        fold_chunk(start, chunk, tok_ref, valid_ref, gain_ref, w_key_ref, w_value_ref,
                   row_tab_ref, col_tab_ref, q_scr, key_scr, val_scr, acc_scr, block_rows)

    def step(k, carry):
        layer = line_place(k, z, length)
        copy(row_of(4 * layer + x_at, core), half, to_x, x_send.at[layer],
             x_recv.at[layer]).wait_recv()
        yd_copy(layer, x_at).start()
        mate_copy(4 * layer + x_at).start()
        copy(row_of(4 * layer + y_at, core), half, to_y, y_send.at[layer],
             y_recv.at[layer]).wait_recv()
        xd_copy(layer, y_at).start()
        mate_copy(4 * layer + y_at).start()

        @pl.when(k < length - 1)
        def _():
            later = line_place(k + 1, z, length)
            copy(row_of(4 * later + me_at, core), half, to_x, x_send.at[later],
                 col_recv.at[later]).wait_recv()
            spread(later)

        @pl.when(k > 0)
        def _():
            mate_wait(4 * layer + me_at)

        mate_wait(4 * layer + x_at)
        fold(pl.multiple_of((4 * layer + 2 * y) * block_rows, chunk))
        yd_copy(layer, d_at).wait_recv()
        xd_copy(layer, d_at).wait_recv()
        mate_copy(4 * layer + d_at).start()
        mate_wait(4 * layer + y_at)
        mate_wait(4 * layer + d_at)
        fold(pl.multiple_of((4 * layer + 2 - 2 * y) * block_rows, chunk))
        return carry

    lax.fori_loop(0, length, step, 0)
    mix_heads(acc_scr, att_scr, block_rows)

    theirs = pl.multiple_of((1 - core) * half, half)
    mine = pl.multiple_of(core * half, half)
    give_scr[...] = jnp.dot(
        att_scr[pl.ds(theirs, half), :], w_out_ref[...], preferred_element_type=jnp.float32
    ).astype(jnp.bfloat16)
    last = pltpu.make_async_remote_copy(
        src_ref=give_scr,
        dst_ref=take_scr,
        send_sem=last_sem.at[0],
        recv_sem=last_sem.at[1],
        device_id=to_mate,
        device_id_type=pl.DeviceIdType.MESH,
    )
    last.start()
    kept = jnp.dot(
        att_scr[pl.ds(mine, half), :], w_out_ref[...], preferred_element_type=jnp.float32
    )

    def settle(layer, carry):
        @pl.when(jnp.logical_and(layer <= z, z < length - 1))
        def _():
            up_copy(layer).wait_send()

        @pl.when(jnp.logical_and(layer >= z, z > 0))
        def _():
            down_copy(layer).wait_send()

        x_copy(layer).wait_send()
        y_copy(layer).wait_send()
        xd_copy(layer, y_at).wait_send()
        yd_copy(layer, x_at).wait_send()
        for at in range(4):
            mate_copy(4 * layer + at).wait_send()
        return carry

    lax.fori_loop(0, length, settle, 0)
    last.wait()
    out_ref[...] = (kept + take_scr[...].astype(jnp.float32)).astype(jnp.bfloat16)


def on_device(tokens, valid_len, norm_gain, w_query, w_key, w_value, q_gain, k_gain, w_out):
    head_width = q_gain.shape[0]
    local_rows, model_width = tokens.shape
    total_sp, total_tp = lax.axis_size("sp"), lax.axis_size("tp")
    block_rows = local_rows * total_tp
    all_rows = block_rows * total_sp
    groups = w_key.shape[1] // head_width
    chunk = CHUNK_BLOCKS * block_rows
    positions = lax.axis_index("sp") * block_rows + jnp.arange(block_rows, dtype=jnp.int32)
    q_factor = HEAD_DIM ** (-0.5) * math.log2(math.e)
    q_tables = with_gain(
        angle_tables(positions // GRID_W, head_width, 0)
        + angle_tables(positions % GRID_W, head_width, 1),
        q_gain, q_factor)
    row_tables = with_gain(
        angle_tables(jnp.arange(all_rows // GRID_W), head_width, 0), k_gain, 1.0)
    col_tables = with_gain(angle_tables(jnp.arange(GRID_W), head_width, 1), k_gain, 1.0)
    gain = norm_gain[None, :]
    vmem = pl.BlockSpec(memory_space=pltpu.VMEM)
    smem = pl.BlockSpec(memory_space=pltpu.SMEM)
    work = [
        pltpu.VMEM((groups, Q_PER_KV * block_rows, head_width), jnp.bfloat16),
        pltpu.VMEM((groups, head_width, chunk), jnp.bfloat16),
        pltpu.VMEM((groups, chunk, 2 * head_width), jnp.bfloat16),
        pltpu.VMEM((groups, Q_PER_KV * block_rows, 2 * head_width), jnp.float32),
        pltpu.VMEM((block_rows, groups * Q_PER_KV * head_width), jnp.bfloat16),
    ]
    if FUSED and total_tp == 2 and total_sp % 4 == 0:
        length = total_sp // 4
        dma = pltpu.SemaphoreType.DMA
        return pl.pallas_call(
            functools.partial(fused_kernel, block_rows, total_sp),
            out_shape=jax.ShapeDtypeStruct((local_rows, model_width), jnp.bfloat16),
            in_specs=[smem] + [vmem] * 9,
            out_specs=vmem,
            scratch_shapes=[pltpu.VMEM((all_rows, model_width), jnp.bfloat16)] + work + [
                pltpu.VMEM((local_rows, model_width), jnp.bfloat16),
                pltpu.VMEM((local_rows, model_width), jnp.bfloat16),
            ] + [dma((length,))] * 5 + [dma((total_sp,))] + [dma((length,))] * 6
            + [dma((total_sp,)), dma((2,))],
            compiler_params=pltpu.CompilerParams(
                collective_id=0, has_side_effects=True, vmem_limit_bytes=60 * 1024 * 1024),
        )(valid_len, tokens, gain, w_query, w_key, w_value, w_out, q_tables, row_tables,
          col_tables)
    gathered = lax.all_gather(tokens, ("sp", "tp"), axis=0, tiled=True)
    own = lax.dynamic_slice_in_dim(gathered, lax.axis_index("sp") * block_rows, block_rows, 0)
    partial = pl.pallas_call(
        functools.partial(local_kernel, block_rows),
        out_shape=jax.ShapeDtypeStruct((block_rows, model_width), jnp.bfloat16),
        in_specs=[smem] + [vmem] * 10,
        out_specs=vmem,
        scratch_shapes=work,
        compiler_params=pltpu.CompilerParams(vmem_limit_bytes=60 * 1024 * 1024),
    )(valid_len, own, gathered, gain, w_query, w_key, w_value, w_out, q_tables, row_tables,
      col_tables)
    return lax.psum_scatter(partial, "tp", scatter_dimension=0, tiled=True)


def solution(mesh):
    return jax.shard_map(
        on_device,
        mesh=mesh,
        in_specs=(
            P(("sp", "tp"), None),
            P(),
            P(),
            P(None, "tp"),
            P(None, "tp"),
            P(None, "tp"),
            P(),
            P(),
            P("tp", None),
        ),
        out_specs=P(("sp", "tp"), None),
        check_vma=False,
    )
```

profile of v0, /device:TPU:1, one launch (start us, length us, event | category | flops | bytes accessed | tf_op | source)
XLA Modules:
  0.0 312.0 jit_solution(1744379019550307503)
XLA Ops:
  6.5 0.0 all-gather.2.cloned.1.call-start
  6.5 0.7 all-gather.2.cloned.1.call-update
  7.3 0.0 reduce-scatter.2.cloned.1.call-start
  7.3 0.1 pad.9.clone
  8.1 0.8 fusion.16
  8.9 0.8 fusion.17
  9.7 0.1 maximum_bitcast_fusion.4
  9.8 0.8 fusion.18
  10.6 0.8 fusion.19
  11.4 0.1 maximum_bitcast_fusion.2
  11.5 0.7 pad_maximum_fusion.8
  12.1 0.7 maximum_multiply_fusion.2
  12.8 0.2 multiply_cosine_fusion.3
  13.0 0.1 pad_bitcast_fusion.3
  13.1 1.5 multiply_cosine_fusion
  14.6 0.1 pad_bitcast_fusion.1
  14.7 0.4 fusion.8
  15.1 0.1 maximum_bitcast_fusion
  15.2 0.6 maximum_multiply_fusion.1.col_tab_ref
  15.9 0.8 maximum_multiply_fusion.row_tab_ref
  16.6 0.8 fusion.q_tab_ref
  17.4 160.5 %all-gather.2.cloned.1.call-done.tok_ref = bf16[16384,1024]{1,0:T(8,128)(2,1)} async-done(((bf16[32,1024]{1,0:T(8,128)(2,1)}), bf16[16384,1024]{1,0:T(8,128)(2,1)}) %all-gather.2.cloned.1.call-update) | async-done | bytes 33554448 | tf_op jit(solution)/shard_map/all_gather | solution.py:381
  177.9 1.9 constant_dynamic-slice_fusion.own_ref
  179.8 94.0 %shard_map.91 = bf16[256,1024]{1,0:T(8,128)(2,1)} custom-call(s32[1]{0:T(128)S(6)} %copy.10.valid_ref, bf16[256,1024]{1,0:T(8,128)(2,1)} %constant_dynamic-slice_fusion.own_ref, bf16[16384,1024]{1,0:T(8,128)(2,1)} %all-gather.2.cloned.1.call-done.tok_ref, f32[1,1024]{1,0:T(1,128)} %bitcast.37, bf16[1024,512]{1,0:T(8,128)(2,1)} %w_query_ref.1, ...), custom_call_target="tpu_custom_call" | custom-call | tf_op jit(solution)/shard_map/pallas_call | solution.py:383
  273.8 0.0 reduce-scatter.2.cloned.1.call-update
  273.8 31.4 %reduce-scatter.2.cloned.1.call-done = bf16[32,1024]{1,0:T(8,128)(2,1)} async-done(((bf16[256,1024]{1,0:T(8,128)(2,1)}), bf16[32,1024]{1,0:T(8,128)(2,1)}) %reduce-scatter.2.cloned.1.call-update) | async-done | bytes 65552 | tf_op jit(solution)/shard_map/reduce_scatter | solution.py:392
  (11 shorter events, 0.1 us)
Async XLA Ops:
  6.5 171.4 %all-gather.2.cloned.1.call-start = ((), (), s32[]{:S(2)}) async-start(), calls=%async_computation.1 | async-start | bytes 33619968 | tf_op jit(solution)/shard_map/all_gather | solution.py:381
  7.3 297.9 %reduce-scatter.2.cloned.1.call-start = ((), (), s32[]{:S(2)}) async-start(), calls=%async_computation.2 | async-start | bytes 589824 | tf_op jit(solution)/shard_map/reduce_scatter | solution.py:392
Sparse Core Ops, SparseCore 0:
  11.8 166.1 all-gather.1
  273.9 31.2 reduce-scatter.1
where the time goes:
time: 313 us; the launch traced here: 312 us
  waiting for transfers between devices  193 us (62%)
  Pallas kernels  94 us (30%)
  between operations  14.2 us (5%)
  other arithmetic  5.86 us (2%)
  local copies, waits for them, and re-layouts  5.38 us (2%)
    all_gather x1, waiting for transfers between devices, on_device(): gathered = lax.all_gather(tokens, ('sp', 'tp'), axis=0, tiled=True)  160 us
    pallas_call x1, Pallas kernels, on_device(): pl.pallas_call(functools.partial(local_kernel, block_rows), out_shape=jax...  94 us
    reduce_scatter x1, waiting for transfers between devices, on_device(): return lax.psum_scatter(partial, 'tp', scatter_dimension=0, tiled=True)  31.4 us
  transfers between devices with their start and end apart: 2, of which 2 were waited for; matrix products, arithmetic and copies ran while one was open for 3% of the time, Pallas kernels for 0%

commit v1 on v0

v1 whole, which is shorter than its diff:
```python
import functools
import math

import jax
import jax.numpy as jnp
from jax import lax
from jax.experimental import pallas as pl
from jax.experimental.pallas import tpu as pltpu
from jax.sharding import PartitionSpec as P

HEAD_DIM = 128
Q_PER_KV = 4
GRID_W = 64
ROWS = 32
BLOCK = 256
HALF = 128
RING = 8
MODEL = 1024

norm_eps = 1e-06
rope_base = 10000.0
MESH = pl.DeviceIdType.MESH


def unit_rows(rows, gain):
    wide = rows.astype(jnp.float32)
    scale = lax.rsqrt(jnp.mean(wide * wide, axis=-1, keepdims=True) + norm_eps)
    return (wide * scale * gain).astype(jnp.bfloat16)


def rotate(part, tables):
    width = part.shape[-1]
    scale = lax.rsqrt(jnp.mean(part * part, axis=-1, keepdims=True) + norm_eps)
    ahead = pltpu.roll(part, width // 4, 1)
    behind = pltpu.roll(part, width - width // 4, 1)
    return (part * tables[0] + ahead * tables[1] + behind * tables[2]) * scale


def kernel(valid_ref, own_ref, gain_ref, gains_ref, w_query_hbm, w_key_hbm, w_value_hbm,
           w_out_hbm, out_ref,
           tok, units, ones, q_scr, acc, att, tabs, w_query, w_key, w_value, w_out,
           give, take, part, landed,
           load_sem, tok_send, tok_recv, unit_recv, near_send, far_send, end_send, end_recv):
    me = lax.axis_index("sp")
    tp = lax.axis_index("tp")
    z, y = me // RING, me % RING
    x, core = tp // 2, tp % 2
    x_up, x_down, x_far = (x + 1) % 4, (x + 3) % 4, (x + 2) % 4
    to_mate = {"sp": me, "tp": 2 * x + 1 - core}

    def along_x(at):
        return {"sp": me, "tp": 2 * at + core}

    to_zy = [
        [{"sp": ((z + 1) % RING) * RING + y, "tp": tp},
         {"sp": ((z + RING - 1) % RING) * RING + y, "tp": tp}],
        [{"sp": z * RING + (y + 1) % RING, "tp": tp},
         {"sp": z * RING + (y + RING - 1) % RING, "tp": tp}],
    ]

    loads = [
        pltpu.make_async_copy(src, dst, load_sem.at[i])
        for i, (src, dst) in enumerate([
            (w_key_hbm, w_key), (w_value_hbm, w_value), (w_query_hbm, w_query),
            (w_out_hbm, w_out)])
    ]
    for load in loads:
        load.start()

    barrier = pltpu.get_barrier_semaphore()
    friends = [to_mate, along_x(x_up), along_x(x_down), along_x(x_far)]
    friends += to_zy[0] + to_zy[1]
    for friend in friends:
        pl.semaphore_signal(barrier, inc=1, device_id=friend, device_id_type=MESH)
    pl.semaphore_wait(barrier, len(friends))

    def remote(source, target, send, recv, device):
        return pltpu.make_async_remote_copy(
            src_ref=source, dst_ref=target, send_sem=send, recv_sem=recv,
            device_id=device, device_id_type=MESH)

    def row_of(at, side):
        return pl.multiple_of(side * HALF + at * ROWS, ROWS)

    def rows_at(at, side):
        return tok.at[pl.ds(row_of(at, side), ROWS), :]

    def half_rows(at, which):
        start = pl.multiple_of(core * HALF + at * ROWS + which * (ROWS // 2), ROWS // 2)
        return tok.at[pl.ds(start, ROWS // 2), :]

    mine = rows_at(x, core)
    tok_up = remote(own_ref, mine, tok_send.at[0], tok_recv.at[0], along_x(x_up))
    tok_down = remote(own_ref, mine, tok_send.at[1], tok_recv.at[1], along_x(x_down))
    tok_mate = remote(own_ref, mine, tok_send.at[2], tok_recv.at[2], to_mate)
    tok_up.start()
    tok_down.start()
    tok_mate.start()
    tok[pl.ds(row_of(x, core), ROWS), :] = own_ref[...]

    lane = lax.broadcasted_iota(jnp.int32, (BLOCK, HEAD_DIM), 1)
    line = lax.broadcasted_iota(jnp.int32, (BLOCK, HEAD_DIM), 0)
    grid_row = me * 4 + (line % HALF) // ROWS
    grid_col = (line // HALF) * ROWS + line % ROWS
    spot = jnp.where(lane < HEAD_DIM // 2, grid_row, grid_col).astype(jnp.float32)
    exponent = (lane % 32).astype(jnp.float32) * (-2.0 / 64 * math.log2(rope_base))
    angle = spot * jnp.exp2(exponent)
    cosine, sine = jnp.cos(angle), jnp.sin(angle)
    second = (lane // 32) % 2 == 1
    tabs[0] = cosine
    tabs[1] = jnp.where(second, sine, 0.0)
    tabs[2] = jnp.where(second, 0.0, -sine)

    valid = valid_ref[0]
    short = lax.broadcasted_iota(jnp.int32, (HALF, HEAD_DIM), 0)
    spread = short + (short // ROWS) * ROWS

    def fill(p, carry):
        for side in range(2):
            kept = spread + (p * BLOCK + side * ROWS) < valid
            ones[2 * p + side] = jnp.where(kept, 1.0, 0.0).astype(jnp.bfloat16)
        return carry

    lax.fori_loop(0, RING * RING, fill, 0)
    acc[...] = jnp.zeros_like(acc)

    fwd_up = remote(half_rows(x_down, 0), half_rows(x_down, 0), tok_send.at[3], tok_recv.at[3],
                    along_x(x_up))
    fwd_down = remote(half_rows(x_up, 1), half_rows(x_up, 1), tok_send.at[4], tok_recv.at[4],
                      along_x(x_down))

    def to_partner(at, slot):
        return remote(rows_at(at, core), rows_at(at, core), tok_send.at[slot],
                      tok_recv.at[slot], to_mate)

    share_down, share_up, share_far = to_partner(x_down, 5), to_partner(x_up, 6), to_partner(x_far, 7)
    tok_up.wait_recv()
    fwd_up.start()
    share_down.start()
    tok_down.wait_recv()
    fwd_down.start()
    share_up.start()
    tok_mate.wait_recv()
    fwd_up.wait_recv()
    fwd_down.wait_recv()
    share_far.start()
    share_down.wait_recv()
    share_up.wait_recv()
    share_far.wait_recv()

    normed = unit_rows(tok[...], gain_ref[...])
    loads[0].wait()
    loads[1].wait()
    turn = [tabs[i] for i in range(3)]
    k_tables = [turn[i] * gains_ref[3 + i:4 + i, :] for i in range(3)]
    keys = rotate(jnp.dot(normed, w_key[...], preferred_element_type=jnp.float32), k_tables)
    values = jnp.dot(normed, w_value[...], preferred_element_type=jnp.float32)
    for side in range(2):
        rows = slice(side * HALF, (side + 1) * HALF)
        kept = spread + (me * BLOCK + side * ROWS) < valid
        units[2 * me + side, :HALF, :] = keys[rows].T.astype(jnp.bfloat16)
        units[2 * me + side, HALF:, :] = jnp.where(kept, values[rows], 0.0).astype(jnp.bfloat16)

    coords = [z, y]

    def unit_at(side, s, t):
        block = s * RING + t if side == 0 else t * RING + s
        return 2 * block + side

    def relay(unit, device, send):
        return remote(units.at[unit], units.at[unit], send, unit_recv.at[unit], device)

    def await_unit(unit):
        remote(units.at[unit], units.at[unit], near_send.at[0], unit_recv.at[unit],
               to_mate).wait_recv()

    def chain(d, sign):
        return jnp.maximum(2 * d - 1 + sign, 0)

    def source(side, d, sign):
        return (coords[side] + d * (2 * sign - 1) + RING) % RING

    def near_copy(side, way, d, unit):
        return relay(unit, to_zy[side][way], near_send.at[(side * 2 + way) * 4 + d])

    def far_copy(side, way, j, k, unit):
        return relay(unit, to_zy[1 - side][way], far_send.at[((side * 2 + way) * 8 + j) * 4 + k])

    def near_sends(side, way, d):
        even = 1 - coords[1 - side] % 2 if way == 0 else coords[1 - side] % 2
        return jnp.logical_or(d < 3, jnp.logical_and(d == 3, even == 1))

    def far_sends(side, way, s, k):
        even = 1 - s % 2 if way == 0 else s % 2
        return jnp.logical_or(k < 3, jnp.logical_and(k == 3, even == 1))

    for side in range(2):
        unit = unit_at(side, coords[side], coords[1 - side])
        for way in range(2):
            near_copy(side, way, 0, unit).start()
            far_copy(side, way, 0, 0, unit).start()

    loads[2].wait()
    q_tables = [turn[i] * gains_ref[i:i + 1, :] for i in range(3)]
    projected = jnp.dot(normed, w_query[...], preferred_element_type=jnp.float32)
    for r in range(Q_PER_KV):
        head = rotate(projected[:, r * HEAD_DIM:(r + 1) * HEAD_DIM], q_tables)
        q_scr[r] = head.astype(jnp.bfloat16)

    def arrive(d, sign):
        for side in range(2):
            unit = unit_at(side, source(side, d, sign), coords[1 - side])
            await_unit(unit)
            for way in range(2):
                far_copy(side, way, chain(d, sign), 0, unit).start()

                @pl.when(jnp.logical_and(sign == way, near_sends(side, way, d)))
                def _():
                    near_copy(side, way, d, unit).start()

    def attend(picks):
        key = jnp.concatenate([units[u, :HALF, :] for u in picks], axis=1)
        val = jnp.concatenate([units[u, HALF:, :] for u in picks], axis=0)
        one = jnp.concatenate([ones[u] for u in picks], axis=0)
        both = jnp.concatenate([val, one], axis=1)
        for r in range(Q_PER_KV):
            scores = jnp.dot(q_scr[r], key, preferred_element_type=jnp.float32)
            weights = jnp.exp2(scores).astype(jnp.bfloat16)
            acc[r] += jnp.dot(weights, both, preferred_element_type=jnp.float32)

    def event(i, state):
        d, sign, k = state

        @pl.when(jnp.logical_and(k == 1, jnp.logical_or(d < 3, jnp.logical_and(d == 3, sign == 0))))
        def _():
            arrive(d + 1, sign)

        @pl.when(jnp.logical_and(k == 1, d == 0))
        def _():
            arrive(d + 1, sign + 1)

        picks = []
        for side in range(2):
            s = source(side, d, sign)
            t = coords[1 - side]
            lower = unit_at(side, s, (t + RING - k) % RING)
            upper = unit_at(side, s, (t + k * (1 - k // 4)) % RING)
            await_unit(lower)

            @pl.when(far_sends(side, 0, s, k))
            def _():
                far_copy(side, 0, chain(d, sign), k, lower).start()

            @pl.when(k < 4)
            def _():
                await_unit(upper)

                @pl.when(far_sends(side, 1, s, k))
                def _():
                    far_copy(side, 1, chain(d, sign), k, upper).start()

            picks += [lower, upper]
        attend(picks)

        flip = jnp.where(jnp.logical_and(sign == 0, jnp.logical_and(d > 0, d < 4)), 1, 0)
        within = jnp.where(jnp.logical_and(d > 0, k < 4), 1, 0)
        top = jnp.minimum(4, d + k)
        d_next = flip * d + (1 - flip) * (within * (d - 1) + (1 - within) * top)
        k_next = flip * k + (1 - flip) * (within * (k + 1) + (1 - within) * (d + k + 1 - top))
        return d_next, flip, k_next

    zero = jnp.int32(0)
    lax.fori_loop(0, 32, event, (zero, zero, zero + 1))

    for r in range(Q_PER_KV):
        att[:, r * HEAD_DIM:(r + 1) * HEAD_DIM] = (
            acc[r, :, :HEAD_DIM] / acc[r, :, HEAD_DIM:]
        ).astype(jnp.bfloat16)

    loads[3].wait()
    theirs = pl.multiple_of((1 - core) * HALF, HALF)
    ours = pl.multiple_of(core * HALF, HALF)
    give[...] = jnp.dot(
        att[pl.ds(theirs, HALF), :], w_out[...], preferred_element_type=jnp.float32
    ).astype(jnp.bfloat16)
    swap = remote(give, take, end_send.at[0], end_recv.at[0], to_mate)
    swap.start()
    kept_sum = jnp.dot(att[pl.ds(ours, HALF), :], w_out[...], preferred_element_type=jnp.float32)
    swap.wait_recv()
    part[...] = kept_sum + take[...].astype(jnp.float32)
    swap.wait_send()
    sends = []
    for i, at in enumerate([x_far, x_up, x_down]):
        here = pl.ds(pl.multiple_of(at * ROWS, ROWS), ROWS)
        give[here, :] = part[here, :].astype(jnp.bfloat16)
        sends.append(remote(give.at[here, :], landed.at[i], end_send.at[1 + i],
                            end_recv.at[1 + i], along_x(at)))
        sends[-1].start()

    for copy in (tok_up, tok_down, tok_mate, fwd_up, fwd_down, share_down, share_up, share_far):
        copy.wait_send()

    def settle(j, carry):
        d = (j + 1) // 2
        sign = jnp.where(j > 0, (j + 1) % 2, 0)
        for side in range(2):
            s = source(side, d, sign)
            unit = unit_at(side, s, coords[1 - side])
            for way in range(2):
                for k in range(4):
                    @pl.when(far_sends(side, way, s, k))
                    def _():
                        far_copy(side, way, j, k, unit).wait_send()

                @pl.when(jnp.logical_and(
                    jnp.logical_or(j == 0, sign == way), near_sends(side, way, d)))
                def _():
                    near_copy(side, way, d, unit).wait_send()
        return carry

    lax.fori_loop(0, 8, settle, 0)
    total = part[pl.ds(pl.multiple_of(x * ROWS, ROWS), ROWS), :]
    for i, copy in enumerate(sends):
        copy.wait_recv()
        total = total + landed[i].astype(jnp.float32)
    for copy in sends:
        copy.wait_send()
    out_ref[...] = total.astype(jnp.bfloat16)


def on_device(tokens, valid_len, norm_gain, w_query, w_key, w_value, q_gain, k_gain, w_out):
    factor = HEAD_DIM ** (-0.5) * math.log2(math.e)

    def three(gain):
        return [gain, jnp.roll(gain, 32), jnp.roll(gain, -32)]

    blank = jnp.zeros_like(q_gain)
    gains = jnp.stack(three(q_gain * factor) + three(k_gain) + [blank, blank])
    vmem = pl.BlockSpec(memory_space=pltpu.VMEM)
    smem = pl.BlockSpec(memory_space=pltpu.SMEM)
    hbm = pl.BlockSpec(memory_space=pl.ANY)
    dma = pltpu.SemaphoreType.DMA
    bf16, f32 = jnp.bfloat16, jnp.float32
    n_units = 2 * RING * RING
    return pl.pallas_call(
        kernel,
        out_shape=jax.ShapeDtypeStruct(tokens.shape, bf16),
        in_specs=[smem, vmem, vmem, vmem, hbm, hbm, hbm, hbm],
        out_specs=vmem,
        scratch_shapes=[
            pltpu.VMEM((BLOCK, MODEL), bf16),
            pltpu.VMEM((n_units, BLOCK, HEAD_DIM), bf16),
            pltpu.VMEM((n_units, HALF, HEAD_DIM), bf16),
            pltpu.VMEM((Q_PER_KV, BLOCK, HEAD_DIM), bf16),
            pltpu.VMEM((Q_PER_KV, BLOCK, 2 * HEAD_DIM), f32),
            pltpu.VMEM((BLOCK, Q_PER_KV * HEAD_DIM), bf16),
            pltpu.VMEM((3, BLOCK, HEAD_DIM), f32),
            pltpu.VMEM(w_query.shape, bf16),
            pltpu.VMEM(w_key.shape, bf16),
            pltpu.VMEM(w_value.shape, bf16),
            pltpu.VMEM(w_out.shape, bf16),
            pltpu.VMEM((HALF, MODEL), bf16),
            pltpu.VMEM((HALF, MODEL), bf16),
            pltpu.VMEM((HALF, MODEL), f32),
            pltpu.VMEM((3, ROWS, MODEL), bf16),
            dma((4,)), dma((8,)), dma((8,)), dma((n_units,)), dma((16,)), dma((128,)),
            dma((4,)), dma((4,)),
        ],
        compiler_params=pltpu.CompilerParams(
            collective_id=0, has_side_effects=True, vmem_limit_bytes=60 * 1024 * 1024),
    )(valid_len, tokens, norm_gain[None, :], gains, w_query, w_key, w_value, w_out)


def solution(mesh):
    return jax.shard_map(
        on_device,
        mesh=mesh,
        in_specs=(
            P(("sp", "tp"), None),
            P(),
            P(),
            P(None, "tp"),
            P(None, "tp"),
            P(None, "tp"),
            P(),
            P(),
            P("tp", None),
        ),
        out_specs=P(("sp", "tp"), None),
        check_vma=False,
    )
```

time: 313 us -> 91.3 us (0.29)
  waiting for transfers between devices: 193 us -> 0 us
  between operations: 14.2 us -> 0.67 us
  Pallas kernels: 94 us -> 86.6 us
  other arithmetic: 5.86 us -> 0.16 us
    all_gather x1 -> x0, waiting for transfers between devices: 160 us -> none  [on_device(): gathered = lax.all_gather(tokens, ('sp', 'tp'), axis=0, tiled=True)]
    reduce_scatter x1 -> x0, waiting for transfers between devices: 31.4 us -> none  [on_device(): return lax.psum_scatter(partial, 'tp', scatter_dimension=0, tiled=True)]
    pallas_call x1, Pallas kernels: 94 us -> 86.6 us  [on_device(): pl.pallas_call(kernel, out_shape=jax.ShapeDtypeStruct(tokens.shape, bf16)...]
  transfers between devices with their start and end apart: 2 -> 0, of which waited for: 2 -> 0; matrix products, arithmetic and copies ran while one was open for 3% -> 0% of each run, Pallas kernels for 0% -> 0%
where the time goes in v1:
time: 91.3 us; the launch traced here: 91.1 us
  Pallas kernels  86.6 us (95%)
  local copies, waits for them, and re-layouts  3.68 us (4%)
    pallas_call x1, Pallas kernels, on_device(): pl.pallas_call(kernel, out_shape=jax.ShapeDtypeStruct(tokens.shape, bf16)...  86.6 us
    unnamed x5, local copies, waits for them, and re-layouts  2.78 us

profile of v1, /device:TPU:1, one launch (start us, length us, event | category | flops | bytes accessed | tf_op | source)
XLA Modules:
  0.0 91.1 jit_solution(15120134720439901025)
XLA Ops:
  0.7 0.0 copy-start.1
  0.7 0.6 copy-done.1
  1.3 0.1 fusion.3
  1.4 0.1 fusion.4
  1.5 0.1 maximum_bitcast_fusion
  1.5 0.0 copy-start
  1.5 0.7 copy-done
  2.2 0.1 fusion.2
  2.3 0.1 fusion.1
  2.3 0.1 maximum_bitcast_fusion.2
  2.4 0.6 stack.31.gains_ref
  3.0 86.6 %shard_map.91 = bf16[32,1024]{1,0:T(8,128)(2,1)} custom-call(s32[1]{0:T(128)S(6)} %copy.11.valid_ref, bf16[32,1024]{1,0:T(8,128)(2,1)} %own_ref.1, f32[1,1024]{1,0:T(1,128)} %bitcast.13, f32[8,128]{1,0:T(8,128)} %stack.31.gains_ref, bf16[1024,512]{1,0:T(8,128)(2,1)} %w_query_hbm.1, bf16[1024,128]{1,0:T(8,128)(2,1)} %w_key_hbm.1, ...), custom_call_target="tpu_custom_call" | custom-call | tf_op jit(solution)/shard_map/pallas_call | solution.py:345
  89.6 1.5 %copy.12 = bf16[32,1024]{1,0:T(8,128)(2,1)} copy(bf16[32,1024]{1,0:T(8,128)(2,1)} %shard_map.91) | data formatting | bytes 131072
  (2 shorter events, 0.0 us)
Async XLA Ops:
  0.7 0.7 copy-start.1
  1.5 0.7 copy-start

commit v2 on v1

v2 whole, which is shorter than its diff:
```python
import functools
import math

import jax
import jax.numpy as jnp
from jax import lax
from jax.experimental import pallas as pl
from jax.experimental.pallas import tpu as pltpu
from jax.sharding import PartitionSpec as P

HEAD_DIM = 128
Q_PER_KV = 4
GRID_W = 64
ROWS = 32
BLOCK = 256
HALF = 128
RING = 8
MODEL = 1024

norm_eps = 1e-06
rope_base = 10000.0
MESH = pl.DeviceIdType.MESH


def unit_rows(rows, gain):
    wide = rows.astype(jnp.float32)
    scale = lax.rsqrt(jnp.mean(wide * wide, axis=-1, keepdims=True) + norm_eps)
    return (wide * scale * gain).astype(jnp.bfloat16)


def rotate(part, tables):
    width = part.shape[-1]
    scale = lax.rsqrt(jnp.mean(part * part, axis=-1, keepdims=True) + norm_eps)
    ahead = pltpu.roll(part, width // 4, 1)
    behind = pltpu.roll(part, width - width // 4, 1)
    return (part * tables[0] + ahead * tables[1] + behind * tables[2]) * scale


def kernel(valid_ref, own_hbm, gain_hbm, q_gain_hbm, k_gain_hbm, w_query_hbm, w_key_hbm,
           w_value_hbm, w_out_hbm, out_ref,
           own, gain, q_gain, k_gain, tok, units, ones, q_scr, acc, att, tabs,
           w_query, w_key, w_value, w_out, o_give, o_take, give, take, part, landed,
           load_sem, tok_send, tok_recv, unit_recv, near_send, far_send, pair_send, pair_recv,
           end_send, end_recv):
    me = lax.axis_index("sp")
    tp = lax.axis_index("tp")
    z, y = me // RING, me % RING
    x, core = tp // 2, tp % 2
    x_up, x_down, x_far = (x + 1) % 4, (x + 3) % 4, (x + 2) % 4
    to_mate = {"sp": me, "tp": 2 * x + 1 - core}
    a = core * y + (1 - core) * z
    b = core * z + (1 - core) * y
    parity, group = a % 2, a // 2

    def block_at(a_at, b_at):
        return (1 - core) * (a_at * RING + b_at) + core * (b_at * RING + a_at)

    def along_x(at):
        return {"sp": me, "tp": 2 * at + core}

    def along(a_at, b_at):
        return {"sp": block_at(a_at, b_at), "tp": tp}

    to_near = [along(2 * ((group + 1) % 4) + parity, b), along(2 * ((group + 3) % 4) + parity, b)]
    to_far = [along(a, (b + 1) % RING), along(a, (b + RING - 1) % RING)]
    to_pair = along(a + 1 - 2 * parity, b)

    barrier = pltpu.get_barrier_semaphore()
    friends = [to_mate, along_x(x_far), along_x(x_up), along_x(x_down), to_pair]
    friends += to_near + to_far
    for friend in friends:
        pl.semaphore_signal(barrier, inc=1, device_id=friend, device_id_type=MESH)

    loads = [
        pltpu.make_async_copy(src, dst, load_sem.at[i])
        for i, (src, dst) in enumerate([
            (own_hbm, own), (gain_hbm, gain), (k_gain_hbm, k_gain), (q_gain_hbm, q_gain),
            (w_key_hbm, w_key), (w_value_hbm, w_value), (w_query_hbm, w_query),
            (w_out_hbm, w_out)])
    ]
    for load in loads:
        load.start()
    loads[0].wait()
    pl.semaphore_wait(barrier, len(friends))

    def remote(source, target, send, recv, device):
        return pltpu.make_async_remote_copy(
            src_ref=source, dst_ref=target, send_sem=send, recv_sem=recv,
            device_id=device, device_id_type=MESH)

    def row_of(at, side):
        return pl.multiple_of(side * HALF + at * ROWS, ROWS)

    def rows_at(at, side):
        return tok.at[pl.ds(row_of(at, side), ROWS), :]

    mine = rows_at(x, core)
    tok_far = remote(own, mine, tok_send.at[0], tok_recv.at[0], along_x(x_far))
    tok_up = remote(own, mine, tok_send.at[1], tok_recv.at[1], along_x(x_up))
    tok_down = remote(own, mine, tok_send.at[2], tok_recv.at[2], along_x(x_down))
    tok_mate = remote(own, mine, tok_send.at[3], tok_recv.at[3], to_mate)
    tok_copies = [tok_far, tok_up, tok_down, tok_mate]
    for copy in tok_copies:
        copy.start()
    tok[pl.ds(row_of(x, core), ROWS), :] = own[...]

    lane = lax.broadcasted_iota(jnp.int32, (BLOCK, HEAD_DIM), 1)
    line = lax.broadcasted_iota(jnp.int32, (BLOCK, HEAD_DIM), 0)
    grid_row = me * 4 + (line % HALF) // ROWS
    grid_col = (line // HALF) * ROWS + line % ROWS
    spot = jnp.where(lane < HEAD_DIM // 2, grid_row, grid_col).astype(jnp.float32)
    exponent = (lane % 32).astype(jnp.float32) * (-2.0 / 64 * math.log2(rope_base))
    angle = spot * jnp.exp2(exponent)
    cosine, sine = jnp.cos(angle), jnp.sin(angle)
    second = (lane // 32) % 2 == 1
    tabs[0] = cosine
    tabs[1] = jnp.where(second, sine, 0.0)
    tabs[2] = jnp.where(second, 0.0, -sine)

    def share(at, slot):
        return remote(rows_at(at, core), rows_at(at, core), tok_send.at[slot],
                      tok_recv.at[slot], to_mate)

    shares = [share(x_far, 4), share(x_down, 5), share(x_up, 6)]
    for copy, onward in ((tok_up, shares[1]), (tok_down, shares[2]), (tok_far, shares[0])):
        copy.wait_recv()
        onward.start()

    valid = valid_ref[0]
    short = lax.broadcasted_iota(jnp.int32, (HALF, HEAD_DIM), 0)
    spread = short + (short // ROWS) * ROWS
    for i in range(1, 6):
        loads[i].wait()

    def turns(table, side):
        wide = jnp.broadcast_to(table, (8, HEAD_DIM))
        moved = [wide, pltpu.roll(wide, 32, 1), pltpu.roll(wide, HEAD_DIM - 32, 1)]
        rows = pl.ds(pl.multiple_of(side * HALF, HALF), HALF)
        return [tabs[i, rows, :] * moved[i][:1, :] for i in range(3)]

    def unit_at(group_at, b_at, side):
        return (group_at * RING + b_at) * 2 + side

    def relay(unit, device, send):
        return remote(units.at[unit], units.at[unit], send, unit_recv.at[unit], device)

    def await_unit(unit):
        relay(unit, to_mate, near_send.at[0]).wait_recv()

    def near_copy(way, d, side, unit):
        return relay(unit, to_near[way], near_send.at[(way * 2 + d) * 2 + side])

    def far_copy(way, j, k, side, unit):
        return relay(unit, to_far[way], far_send.at[((way * 4 + j) * 4 + k) * 2 + side])

    def project(side):
        rows = pl.ds(pl.multiple_of(side * HALF, HALF), HALF)
        normed = unit_rows(tok[rows, :], gain[...])
        keys = rotate(jnp.dot(normed, w_key[...], preferred_element_type=jnp.float32),
                      turns(k_gain[...], side))
        values = jnp.dot(normed, w_value[...], preferred_element_type=jnp.float32)
        kept = spread + (me * BLOCK + side * ROWS) < valid
        unit = unit_at(group, b, side)
        units[unit, :HALF, :] = keys.T.astype(jnp.bfloat16)
        units[unit, HALF:, :] = jnp.where(kept, values, 0.0).astype(jnp.bfloat16)
        for way in range(2):
            far_copy(way, 0, 0, side, unit).start()
            near_copy(way, 0, side, unit).start()
        return normed

    def queries(normed, side):
        rows = pl.ds(pl.multiple_of(side * HALF, HALF), HALF)
        factor = HEAD_DIM ** (-0.5) * math.log2(math.e)
        tables = turns(q_gain[...] * factor, side)
        projected = jnp.dot(normed, w_query[...], preferred_element_type=jnp.float32)
        for r in range(Q_PER_KV):
            head = rotate(projected[:, r * HEAD_DIM:(r + 1) * HEAD_DIM], tables)
            q_scr[r, rows, :] = head.astype(jnp.bfloat16)

    first = project(core)
    tok_mate.wait_recv()
    for copy in shares:
        copy.wait_recv()
    other = project(1 - core)
    loads[6].wait()
    queries(first, core)
    queries(other, 1 - core)
    q_swap = remote(q_scr.at[pl.ds(0, 4)], q_scr.at[pl.ds(4, 4)], pair_send.at[0],
                    pair_recv.at[0], to_pair)
    q_swap.start()

    def fill(i, carry):
        p = block_at(2 * (i // RING) + parity, i % RING)
        for side in range(2):
            kept = spread + (p * BLOCK + side * ROWS) < valid
            ones[2 * i + side] = jnp.where(kept, 1.0, 0.0).astype(jnp.bfloat16)
        return carry

    lax.fori_loop(0, 4 * RING, fill, 0)
    acc[...] = jnp.zeros_like(acc)

    def chain(d, sign):
        return jnp.maximum(2 * d - 1 + sign, 0)

    def source(d, sign):
        return (group + d * (2 * sign - 1) + 4) % 4

    def arrive(d, sign):
        for side in range(2):
            unit = unit_at(source(d, sign), b, side)
            await_unit(unit)
            for way in range(2):
                far_copy(way, chain(d, sign), 0, side, unit).start()

            @pl.when(jnp.logical_and(d == 1, sign == side))
            def _():
                near_copy(side, 1, side, unit).start()

    def attend(picks, heads):
        key = jnp.concatenate([units[u, :HALF, :] for u in picks], axis=1)
        val = jnp.concatenate([units[u, HALF:, :] for u in picks], axis=0)
        one = jnp.concatenate([ones[u] for u in picks], axis=0)
        both = jnp.concatenate([val, one], axis=1)
        for r in heads:
            scores = jnp.dot(q_scr[r], key, preferred_element_type=jnp.float32)
            weights = jnp.exp2(scores).astype(jnp.bfloat16)
            acc[r] += jnp.dot(weights, both, preferred_element_type=jnp.float32)

    def event(i, state):
        d, sign, k = state

        @pl.when(jnp.logical_and(k == 1, jnp.logical_and(d < 2, sign == 0)))
        def _():
            arrive(d + 1, sign)

        @pl.when(jnp.logical_and(k == 1, d == 0))
        def _():
            arrive(d + 1, sign + 1)

        s = source(d, sign)
        low, high = (b + RING - k) % RING, (b + k) % RING
        for side in range(2):
            for way, at in enumerate((low, high)):
                unit = unit_at(s, at, side)

                @pl.when(jnp.logical_or(k < 4, side == way))
                def _():
                    await_unit(unit)

                @pl.when(jnp.logical_or(k < 3, jnp.logical_and(k == 3, side == way)))
                def _():
                    far_copy(way, chain(d, sign), k, side, unit).start()

        last = k // 4
        second = last * b + (1 - last) * high
        picks = [unit_at(s, at, side) for at in (low, second) for side in range(2)]

        @pl.when(i == 0)
        def _():
            q_swap.wait_recv()

        attend(picks, range(8))

        flip = jnp.where(jnp.logical_and(sign == 0, d == 1), 1, 0)
        within = jnp.where(jnp.logical_and(d > 0, k < 4), 1, 0)
        top = jnp.minimum(2, d + k)
        d_next = flip * d + (1 - flip) * (within * (d - 1) + (1 - within) * top)
        k_next = flip * k + (1 - flip) * (within * (k + 1) + (1 - within) * (d + k + 1 - top))
        return d_next, flip, k_next

    zero = jnp.int32(0)
    lax.fori_loop(0, 16, event, (zero, zero, zero + 1))

    small = lax.broadcasted_iota(jnp.int32, (BLOCK, HEAD_DIM), 1) // 32
    sums = acc[4, :, HEAD_DIM:]
    for r in range(Q_PER_KV):
        o_give[:, r * HEAD_DIM:(r + 1) * HEAD_DIM] = acc[4 + r, :, :HEAD_DIM].astype(jnp.bfloat16)
        sums = jnp.where(small == r, acc[4 + r, :, HEAD_DIM:], sums)
    o_give[:, 4 * HEAD_DIM:] = sums.astype(jnp.bfloat16)
    o_swap = remote(o_give, o_take, pair_send.at[1], pair_recv.at[1], to_pair)
    o_swap.start()

    def settle(j, carry):
        d = (j + 1) // 2
        sign = jnp.where(j > 0, (j + 1) % 2, 0)
        s = source(d, sign)
        for side in range(2):
            unit = unit_at(s, b, side)
            for way in range(2):
                for k in range(4 if side == way else 3):
                    far_copy(way, j, k, side, unit).wait_send()

                @pl.when(j == 0)
                def _():
                    near_copy(way, 0, side, unit).wait_send()

            @pl.when(jnp.logical_and(d == 1, sign == side))
            def _():
                near_copy(side, 1, side, unit).wait_send()
        return carry

    lax.fori_loop(0, 4, settle, 0)
    for copy in tok_copies + shares + [q_swap]:
        copy.wait_send()
    loads[7].wait()
    o_swap.wait_recv()
    for r in range(Q_PER_KV):
        span = slice(r * HEAD_DIM, (r + 1) * HEAD_DIM)
        total = acc[r, :, HEAD_DIM:] + o_take[
            :, 4 * HEAD_DIM + 32 * r:4 * HEAD_DIM + 32 * r + 1].astype(jnp.float32)
        att[:, span] = (
            (acc[r, :, :HEAD_DIM] + o_take[:, span].astype(jnp.float32)) / total
        ).astype(jnp.bfloat16)

    theirs = pl.multiple_of((1 - core) * HALF, HALF)
    ours = pl.multiple_of(core * HALF, HALF)
    give[...] = jnp.dot(
        att[pl.ds(theirs, HALF), :], w_out[...], preferred_element_type=jnp.float32
    ).astype(jnp.bfloat16)
    swap = remote(give, take, end_send.at[0], end_recv.at[0], to_mate)
    swap.start()
    kept_sum = jnp.dot(att[pl.ds(ours, HALF), :], w_out[...], preferred_element_type=jnp.float32)
    swap.wait_recv()
    part[...] = kept_sum + take[...].astype(jnp.float32)
    swap.wait_send()
    sends = []
    for i, at in enumerate([x_far, x_up, x_down]):
        here = pl.ds(pl.multiple_of(at * ROWS, ROWS), ROWS)
        give[here, :] = part[here, :].astype(jnp.bfloat16)
        sends.append(remote(give.at[here, :], landed.at[i], end_send.at[1 + i],
                            end_recv.at[1 + i], along_x(at)))
        sends[-1].start()

    total = part[pl.ds(pl.multiple_of(x * ROWS, ROWS), ROWS), :]
    o_swap.wait_send()
    for i, copy in enumerate(sends):
        copy.wait_recv()
        total = total + landed[i].astype(jnp.float32)
    for copy in sends:
        copy.wait_send()
    out_ref[...] = total.astype(jnp.bfloat16)


def on_device(tokens, valid_len, norm_gain, w_query, w_key, w_value, q_gain, k_gain, w_out):
    vmem = pl.BlockSpec(memory_space=pltpu.VMEM)
    smem = pl.BlockSpec(memory_space=pltpu.SMEM)
    hbm = pl.BlockSpec(memory_space=pl.ANY)
    dma = pltpu.SemaphoreType.DMA
    bf16, f32 = jnp.bfloat16, jnp.float32
    n_units = RING * RING
    return pl.pallas_call(
        kernel,
        out_shape=jax.ShapeDtypeStruct(tokens.shape, bf16),
        in_specs=[smem] + [hbm] * 8,
        out_specs=vmem,
        scratch_shapes=[
            pltpu.VMEM(tokens.shape, bf16),
            pltpu.VMEM((1, MODEL), f32),
            pltpu.VMEM((1, HEAD_DIM), f32),
            pltpu.VMEM((1, HEAD_DIM), f32),
            pltpu.VMEM((BLOCK, MODEL), bf16),
            pltpu.VMEM((n_units, BLOCK, HEAD_DIM), bf16),
            pltpu.VMEM((n_units, HALF, HEAD_DIM), bf16),
            pltpu.VMEM((2 * Q_PER_KV, BLOCK, HEAD_DIM), bf16),
            pltpu.VMEM((2 * Q_PER_KV, BLOCK, 2 * HEAD_DIM), f32),
            pltpu.VMEM((BLOCK, Q_PER_KV * HEAD_DIM), bf16),
            pltpu.VMEM((3, BLOCK, HEAD_DIM), f32),
            pltpu.VMEM(w_query.shape, bf16),
            pltpu.VMEM(w_key.shape, bf16),
            pltpu.VMEM(w_value.shape, bf16),
            pltpu.VMEM(w_out.shape, bf16),
            pltpu.VMEM((BLOCK, 5 * HEAD_DIM), bf16),
            pltpu.VMEM((BLOCK, 5 * HEAD_DIM), bf16),
            pltpu.VMEM((HALF, MODEL), bf16),
            pltpu.VMEM((HALF, MODEL), bf16),
            pltpu.VMEM((HALF, MODEL), f32),
            pltpu.VMEM((3, ROWS, MODEL), bf16),
            dma((8,)), dma((8,)), dma((8,)), dma((n_units,)), dma((8,)), dma((64,)),
            dma((2,)), dma((2,)), dma((4,)), dma((4,)),
        ],
        compiler_params=pltpu.CompilerParams(
            collective_id=0, has_side_effects=True, vmem_limit_bytes=60 * 1024 * 1024),
    )(valid_len, tokens, norm_gain[None, :], q_gain[None, :], k_gain[None, :], w_query, w_key,
      w_value, w_out)


def solution(mesh):
    return jax.shard_map(
        on_device,
        mesh=mesh,
        in_specs=(
            P(("sp", "tp"), None),
            P(),
            P(),
            P(None, "tp"),
            P(None, "tp"),
            P(None, "tp"),
            P(),
            P(),
            P("tp", None),
        ),
        out_specs=P(("sp", "tp"), None),
        check_vma=False,
    )
```

time: 91.3 us -> 71.9 us (0.79)
  Pallas kernels: 86.6 us -> 69.5 us
  local copies, waits for them, and re-layouts: 3.68 us -> 1.47 us
    pallas_call x1, Pallas kernels: 86.6 us -> 69.5 us  [on_device(): pl.pallas_call(kernel, out_shape=jax.ShapeDtypeStruct(tokens.shape, bf16)...]
    unnamed x5 -> x1, local copies, waits for them, and re-layouts: 2.78 us -> 1.47 us
where the time goes in v2:
time: 71.9 us; the launch traced here: 71.7 us
  Pallas kernels  69.5 us (97%)
  local copies, waits for them, and re-layouts  1.47 us (2%)
    pallas_call x1, Pallas kernels, on_device(): pl.pallas_call(kernel, out_shape=jax.ShapeDtypeStruct(tokens.shape, bf16)...  69.5 us
    unnamed x1, local copies, waits for them, and re-layouts  1.47 us

profile of v2, /device:TPU:1, one launch (start us, length us, event | category | flops | bytes accessed | tf_op | source)
XLA Modules:
  0.0 71.7 jit_solution(15924857987300183679)
XLA Ops:
  0.7 69.5 %shard_map.91 = bf16[32,1024]{1,0:T(8,128)(2,1)} custom-call(s32[1]{0:T(128)S(6)} %copy.11.valid_ref, bf16[32,1024]{1,0:T(8,128)(2,1)} %own_hbm.1, f32[1,1024]{1,0:T(1,128)} %bitcast.3, f32[1,128]{1,0:T(1,128)} %bitcast.4, f32[1,128]{1,0:T(1,128)} %bitcast.5, bf16[1024,512]{1,0:T(8,128)(2,1)} %w_query_hbm.1, bf16[1024,128]{1,0:T(8,128)(2,1)} %w_key_hbm.1, ...), custom_call_target="tpu_custom_call" | custom-call | tf_op jit(solution)/shard_map/pallas_call | solution.py:351
  70.2 1.5 %copy.12 = bf16[32,1024]{1,0:T(8,128)(2,1)} copy(bf16[32,1024]{1,0:T(8,128)(2,1)} %shard_map.91) | data formatting | bytes 131072

commit v3 on v2

--- a/solution.py
+++ b/solution.py
@@ -17,6 +17,14 @@
 RING = 8
 MODEL = 1024
 
+LATE = 6
+ORDER = [
+    (0, 0, 1, 1), (1, 1, 1, 2), (1, 0, 1, 0), (0, 0, 2, 0),
+    (2, 0, 1, 0), (1, 1, 2, 0), (1, 0, 2, 0), (0, 0, 3, 0),
+    (2, 0, 2, 0), (1, 1, 3, 0), (1, 0, 3, 0), (0, 0, 4, 0),
+    (2, 0, 3, 0), (1, 1, 4, 0), (1, 0, 4, 0), (2, 0, 4, 0),
+]
+
 norm_eps = 1e-06
 rope_base = 10000.0
 MESH = pl.DeviceIdType.MESH
@@ -39,7 +47,7 @@
 def kernel(valid_ref, own_hbm, gain_hbm, q_gain_hbm, k_gain_hbm, w_query_hbm, w_key_hbm,
            w_value_hbm, w_out_hbm, out_ref,
            own, gain, q_gain, k_gain, tok, units, ones, q_scr, acc, att, tabs,
-           w_query, w_key, w_value, w_out, o_give, o_take, give, take, part, landed,
+           w_query, w_key, w_value, w_out, o_give, o_take, give, take, ship, landed,
            load_sem, tok_send, tok_recv, unit_recv, near_send, far_send, pair_send, pair_recv,
            end_send, end_recv):
     me = lax.axis_index("sp")
@@ -88,27 +96,30 @@
             src_ref=source, dst_ref=target, send_sem=send, recv_sem=recv,
             device_id=device, device_id_type=MESH)
 
-    def row_of(at, side):
-        return pl.multiple_of(side * HALF + at * ROWS, ROWS)
-
-    def rows_at(at, side):
-        return tok.at[pl.ds(row_of(at, side), ROWS), :]
-
-    mine = rows_at(x, core)
-    tok_far = remote(own, mine, tok_send.at[0], tok_recv.at[0], along_x(x_far))
-    tok_up = remote(own, mine, tok_send.at[1], tok_recv.at[1], along_x(x_up))
-    tok_down = remote(own, mine, tok_send.at[2], tok_recv.at[2], along_x(x_down))
-    tok_mate = remote(own, mine, tok_send.at[3], tok_recv.at[3], to_mate)
-    tok_copies = [tok_far, tok_up, tok_down, tok_mate]
+    def slot(at):
+        return tok.at[at * ROWS:(at + 1) * ROWS, :]
+
+    tok_up = remote(own, slot(2), tok_send.at[0], tok_recv.at[0], along_x(x_up))
+    tok_down = remote(own, slot(1), tok_send.at[1], tok_recv.at[1], along_x(x_down))
+    tok_mate = remote(own, slot(0), tok_send.at[2], tok_recv.at[2], to_mate)
+    tok_far = remote(own, slot(4), tok_send.at[3], tok_recv.at[3], along_x(x_far))
+    tok_copies = [tok_up, tok_down, tok_mate, tok_far]
     for copy in tok_copies:
         copy.start()
-    tok[pl.ds(row_of(x, core), ROWS), :] = own[...]
+    tok[3 * ROWS:4 * ROWS, :] = own[...]
+
+    def place(line):
+        at = line // ROWS
+        ahead = jnp.where(jnp.logical_or(at == 1, at == 6), 1, 0)
+        ahead = jnp.where(jnp.logical_or(at == 2, at == 7), 3, ahead)
+        ahead = jnp.where(jnp.logical_or(at == 4, at == 5), 2, ahead)
+        side = jnp.where(jnp.logical_and(at > 0, at < 5), core, 1 - core)
+        return (x + ahead) % 4, side * ROWS + line % ROWS
 
     lane = lax.broadcasted_iota(jnp.int32, (BLOCK, HEAD_DIM), 1)
     line = lax.broadcasted_iota(jnp.int32, (BLOCK, HEAD_DIM), 0)
-    grid_row = me * 4 + (line % HALF) // ROWS
-    grid_col = (line // HALF) * ROWS + line % ROWS
-    spot = jnp.where(lane < HEAD_DIM // 2, grid_row, grid_col).astype(jnp.float32)
+    grid_row, grid_col = place(line)
+    spot = jnp.where(lane < HEAD_DIM // 2, me * 4 + grid_row, grid_col).astype(jnp.float32)
     exponent = (lane % 32).astype(jnp.float32) * (-2.0 / 64 * math.log2(rope_base))
     angle = spot * jnp.exp2(exponent)
     cosine, sine = jnp.cos(angle), jnp.sin(angle)
@@ -117,25 +128,38 @@
     tabs[1] = jnp.where(second, sine, 0.0)
     tabs[2] = jnp.where(second, 0.0, -sine)
 
-    def share(at, slot):
-        return remote(rows_at(at, core), rows_at(at, core), tok_send.at[slot],
-                      tok_recv.at[slot], to_mate)
-
-    shares = [share(x_far, 4), share(x_down, 5), share(x_up, 6)]
-    for copy, onward in ((tok_up, shares[1]), (tok_down, shares[2]), (tok_far, shares[0])):
+    valid = valid_ref[0]
+    spread = []
+    for side in range(2):
+        short = lax.broadcasted_iota(jnp.int32, (HALF, HEAD_DIM), 0) + side * HALF
+        high, low = place(short)
+        spread.append(high * GRID_W + low)
+    def fill(i, carry):
+        p = block_at(2 * (i // RING) + parity, i % RING)
+        for side in range(2):
+            kept = spread[side] + p * BLOCK < valid
+            ones[2 * i + side] = jnp.where(kept, 1.0, 0.0).astype(jnp.bfloat16)
+        return carry
+
+    lax.fori_loop(0, 4 * RING, fill, 0)
+    acc[...] = jnp.zeros_like(acc)
+
+    def share(ours, theirs, at):
+        return remote(slot(ours), slot(theirs), tok_send.at[at], tok_recv.at[at], to_mate)
+
+    shares = [share(2, 7, 4), share(1, 6, 5), share(4, 5, 6)]
+    for copy, onward in zip((tok_up, tok_down), shares):
         copy.wait_recv()
         onward.start()
-
-    valid = valid_ref[0]
-    short = lax.broadcasted_iota(jnp.int32, (HALF, HEAD_DIM), 0)
-    spread = short + (short // ROWS) * ROWS
+    tok_mate.wait_recv()
+
     for i in range(1, 6):
         loads[i].wait()
 
     def turns(table, side):
         wide = jnp.broadcast_to(table, (8, HEAD_DIM))
         moved = [wide, pltpu.roll(wide, 32, 1), pltpu.roll(wide, HEAD_DIM - 32, 1)]
-        rows = pl.ds(pl.multiple_of(side * HALF, HALF), HALF)
+        rows = slice(side * HALF, (side + 1) * HALF)
         return [tabs[i, rows, :] * moved[i][:1, :] for i in range(3)]
 
     def unit_at(group_at, b_at, side):
@@ -154,12 +178,12 @@
         return relay(unit, to_far[way], far_send.at[((way * 4 + j) * 4 + k) * 2 + side])
 
     def project(side):
-        rows = pl.ds(pl.multiple_of(side * HALF, HALF), HALF)
+        rows = slice(side * HALF, (side + 1) * HALF)
         normed = unit_rows(tok[rows, :], gain[...])
         keys = rotate(jnp.dot(normed, w_key[...], preferred_element_type=jnp.float32),
                       turns(k_gain[...], side))
         values = jnp.dot(normed, w_value[...], preferred_element_type=jnp.float32)
-        kept = spread + (me * BLOCK + side * ROWS) < valid
+        kept = spread[side] + me * BLOCK < valid
         unit = unit_at(group, b, side)
         units[unit, :HALF, :] = keys.T.astype(jnp.bfloat16)
         units[unit, HALF:, :] = jnp.where(kept, values, 0.0).astype(jnp.bfloat16)
@@ -169,7 +193,7 @@
         return normed
 
     def queries(normed, side):
-        rows = pl.ds(pl.multiple_of(side * HALF, HALF), HALF)
+        rows = slice(side * HALF, (side + 1) * HALF)
         factor = HEAD_DIM ** (-0.5) * math.log2(math.e)
         tables = turns(q_gain[...] * factor, side)
         projected = jnp.dot(normed, w_query[...], preferred_element_type=jnp.float32)
@@ -177,27 +201,18 @@
             head = rotate(projected[:, r * HEAD_DIM:(r + 1) * HEAD_DIM], tables)
             q_scr[r, rows, :] = head.astype(jnp.bfloat16)
 
-    first = project(core)
-    tok_mate.wait_recv()
+    first = project(0)
+    tok_far.wait_recv()
+    shares[2].start()
     for copy in shares:
         copy.wait_recv()
-    other = project(1 - core)
+    other = project(1)
     loads[6].wait()
-    queries(first, core)
-    queries(other, 1 - core)
+    queries(first, 0)
+    queries(other, 1)
     q_swap = remote(q_scr.at[pl.ds(0, 4)], q_scr.at[pl.ds(4, 4)], pair_send.at[0],
                     pair_recv.at[0], to_pair)
     q_swap.start()
-
-    def fill(i, carry):
-        p = block_at(2 * (i // RING) + parity, i % RING)
-        for side in range(2):
-            kept = spread + (p * BLOCK + side * ROWS) < valid
-            ones[2 * i + side] = jnp.where(kept, 1.0, 0.0).astype(jnp.bfloat16)
-        return carry
-
-    lax.fori_loop(0, 4 * RING, fill, 0)
-    acc[...] = jnp.zeros_like(acc)
 
     def chain(d, sign):
         return jnp.maximum(2 * d - 1 + sign, 0)
@@ -212,8 +227,7 @@
             for way in range(2):
                 far_copy(way, chain(d, sign), 0, side, unit).start()
 
-            @pl.when(jnp.logical_and(d == 1, sign == side))
-            def _():
+            if d == 1 and sign == side:
                 near_copy(side, 1, side, unit).start()
 
     def attend(picks, heads):
@@ -221,24 +235,35 @@
         val = jnp.concatenate([units[u, HALF:, :] for u in picks], axis=0)
         one = jnp.concatenate([ones[u] for u in picks], axis=0)
         both = jnp.concatenate([val, one], axis=1)
-        for r in heads:
-            scores = jnp.dot(q_scr[r], key, preferred_element_type=jnp.float32)
-            weights = jnp.exp2(scores).astype(jnp.bfloat16)
+        def score(r):
+            return jnp.dot(q_scr[r], key, preferred_element_type=jnp.float32)
+
+        heads = list(heads)
+        ahead = score(heads[0])
+        for at, r in enumerate(heads):
+            weights = jnp.exp2(ahead).astype(jnp.bfloat16)
+            if at + 1 < len(heads):
+                ahead = score(heads[at + 1])
             acc[r] += jnp.dot(weights, both, preferred_element_type=jnp.float32)
 
-    def event(i, state):
-        d, sign, k = state
-
-        @pl.when(jnp.logical_and(k == 1, jnp.logical_and(d < 2, sign == 0)))
-        def _():
-            arrive(d + 1, sign)
-
-        @pl.when(jnp.logical_and(k == 1, d == 0))
-        def _():
-            arrive(d + 1, sign + 1)
-
-        s = source(d, sign)
-        low, high = (b + RING - k) % RING, (b + k) % RING
+    def lookup(i):
+        code = jnp.int32(0)
+        for at, (d, sign, k, step) in enumerate(ORDER):
+            code = jnp.where(i == at, ((d * 2 + sign) * 5 + k) * 4 + step, code)
+        step, rest = code % 4, code // 4
+        k, rest = rest % 5, rest // 5
+        return rest // 2, rest % 2, k, step
+
+    def picks_of(i):
+        d, sign, k, step = lookup(i)
+        s, low, high = source(d, sign), (b + RING - k) % RING, (b + k) % RING
+        last = k // 4
+        second = last * b + (1 - last) * high
+        return [unit_at(s, at, side) for at in (low, second) for side in range(2)]
+
+    def exchange(i):
+        d, sign, k, step = lookup(i)
+        s, low, high = source(d, sign), (b + RING - k) % RING, (b + k) % RING
         for side in range(2):
             for way, at in enumerate((low, high)):
                 unit = unit_at(s, at, side)
@@ -251,25 +276,32 @@
                 def _():
                     far_copy(way, chain(d, sign), k, side, unit).start()
 
-        last = k // 4
-        second = last * b + (1 - last) * high
-        picks = [unit_at(s, at, side) for at in (low, second) for side in range(2)]
+        @pl.when(step == 1)
+        def _():
+            arrive(1, 1)
+            arrive(1, 0)
+
+        @pl.when(step == 2)
+        def _():
+            arrive(2, 0)
+
+    def event(i, carry):
+        exchange(i)
 
         @pl.when(i == 0)
         def _():
             q_swap.wait_recv()
 
-        attend(picks, range(8))
-
-        flip = jnp.where(jnp.logical_and(sign == 0, d == 1), 1, 0)
-        within = jnp.where(jnp.logical_and(d > 0, k < 4), 1, 0)
-        top = jnp.minimum(2, d + k)
-        d_next = flip * d + (1 - flip) * (within * (d - 1) + (1 - within) * top)
-        k_next = flip * k + (1 - flip) * (within * (k + 1) + (1 - within) * (d + k + 1 - top))
-        return d_next, flip, k_next
-
-    zero = jnp.int32(0)
-    lax.fori_loop(0, 16, event, (zero, zero, zero + 1))
+        attend(picks_of(i), range(8))
+        return carry
+
+    def late_event(i, carry):
+        exchange(i)
+        attend(picks_of(i), range(4, 8))
+        return carry
+
+    lax.fori_loop(0, 16 - LATE, event, 0)
+    lax.fori_loop(16 - LATE, 16, late_event, 0)
 
     small = lax.broadcasted_iota(jnp.int32, (BLOCK, HEAD_DIM), 1) // 32
     sums = acc[4, :, HEAD_DIM:]
@@ -277,8 +309,13 @@
         o_give[:, r * HEAD_DIM:(r + 1) * HEAD_DIM] = acc[4 + r, :, :HEAD_DIM].astype(jnp.bfloat16)
         sums = jnp.where(small == r, acc[4 + r, :, HEAD_DIM:], sums)
     o_give[:, 4 * HEAD_DIM:] = sums.astype(jnp.bfloat16)
-    o_swap = remote(o_give, o_take, pair_send.at[1], pair_recv.at[1], to_pair)
-    o_swap.start()
+    o_swaps = [
+        remote(o_give.at[low:high, :], o_take.at[low:high, :], pair_send.at[at],
+               pair_recv.at[at], to_pair)
+        for at, (low, high) in enumerate(((128, 192), (192, 256), (0, 128)), 1)
+    ]
+    for copy in o_swaps:
+        copy.start()
 
     def settle(j, carry):
         d = (j + 1) // 2
@@ -299,44 +336,74 @@
                 near_copy(side, 1, side, unit).wait_send()
         return carry
 
+    def catch_up(i, carry):
+        first = 16 - LATE + 2 * i
+        attend(picks_of(first) + picks_of(first + 1), range(4))
+        return carry
+
+    lax.fori_loop(0, LATE // 2, catch_up, 0)
     lax.fori_loop(0, 4, settle, 0)
     for copy in tok_copies + shares + [q_swap]:
         copy.wait_send()
     loads[7].wait()
-    o_swap.wait_recv()
-    for r in range(Q_PER_KV):
-        span = slice(r * HEAD_DIM, (r + 1) * HEAD_DIM)
-        total = acc[r, :, HEAD_DIM:] + o_take[
-            :, 4 * HEAD_DIM + 32 * r:4 * HEAD_DIM + 32 * r + 1].astype(jnp.float32)
-        att[:, span] = (
-            (acc[r, :, :HEAD_DIM] + o_take[:, span].astype(jnp.float32)) / total
-        ).astype(jnp.bfloat16)
-
-    theirs = pl.multiple_of((1 - core) * HALF, HALF)
-    ours = pl.multiple_of(core * HALF, HALF)
-    give[...] = jnp.dot(
-        att[pl.ds(theirs, HALF), :], w_out[...], preferred_element_type=jnp.float32
-    ).astype(jnp.bfloat16)
-    swap = remote(give, take, end_send.at[0], end_recv.at[0], to_mate)
+
+    def combine(low, high):
+        rows = slice(low, high)
+        for r in range(Q_PER_KV):
+            span = slice(r * HEAD_DIM, (r + 1) * HEAD_DIM)
+            lane_at = 4 * HEAD_DIM + 32 * r
+            total = acc[r, rows, HEAD_DIM:] + o_take[
+                rows, lane_at:lane_at + 1].astype(jnp.float32)
+            att[rows, span] = (
+                (acc[r, rows, :HEAD_DIM] + o_take[rows, span].astype(jnp.float32)) / total
+            ).astype(jnp.bfloat16)
+
+    def mix(low, high):
+        return jnp.dot(att[low * ROWS:high * ROWS, :], w_out[...],
+                       preferred_element_type=jnp.float32)
+
+    def part_of(ref, low, high):
+        return ref.at[low * ROWS:high * ROWS, :]
+
+    o_swaps[0].wait_recv()
+    combine(128, 192)
+    both = mix(4, 6)
+    give[3 * ROWS:, :] = both[ROWS:].astype(jnp.bfloat16)
+    swap_far = remote(part_of(give, 3, 4), part_of(take, 3, 4), end_send.at[0],
+                      end_recv.at[0], to_mate)
+    swap_far.start()
+    swap_far.wait_recv()
+    ship[2 * ROWS:, :] = (both[:ROWS] + take[3 * ROWS:, :].astype(jnp.float32)).astype(jnp.bfloat16)
+    out_far = remote(part_of(ship, 2, 3), landed.at[0], end_send.at[1], end_recv.at[1],
+                     along_x(x_far))
+    out_far.start()
+
+    o_swaps[1].wait_recv()
+    combine(192, 256)
+    give[:2 * ROWS, :] = mix(6, 8).astype(jnp.bfloat16)
+    o_swaps[2].wait_recv()
+    combine(0, 128)
+    front = mix(0, 4)
+    give[2 * ROWS:3 * ROWS, :] = front[:ROWS].astype(jnp.bfloat16)
+    swap = remote(part_of(give, 0, 3), part_of(take, 0, 3), end_send.at[2], end_recv.at[2],
+                  to_mate)
     swap.start()
-    kept_sum = jnp.dot(att[pl.ds(ours, HALF), :], w_out[...], preferred_element_type=jnp.float32)
     swap.wait_recv()
-    part[...] = kept_sum + take[...].astype(jnp.float32)
-    swap.wait_send()
-    sends = []
-    for i, at in enumerate([x_far, x_up, x_down]):
-        here = pl.ds(pl.multiple_of(at * ROWS, ROWS), ROWS)
-        give[here, :] = part[here, :].astype(jnp.bfloat16)
-        sends.append(remote(give.at[here, :], landed.at[i], end_send.at[1 + i],
-                            end_recv.at[1 + i], along_x(at)))
-        sends[-1].start()
-
-    total = part[pl.ds(pl.multiple_of(x * ROWS, ROWS), ROWS), :]
-    o_swap.wait_send()
-    for i, copy in enumerate(sends):
+    near = front[ROWS:] + take[:3 * ROWS, :].astype(jnp.float32)
+    ship[:2 * ROWS, :] = near[:2 * ROWS].astype(jnp.bfloat16)
+    out_up = remote(part_of(ship, 0, 1), landed.at[1], end_send.at[3], end_recv.at[3],
+                    along_x(x_up))
+    out_down = remote(part_of(ship, 1, 2), landed.at[2], end_send.at[4], end_recv.at[4],
+                      along_x(x_down))
+    out_up.start()
+    out_down.start()
+    total = near[2 * ROWS:]
+    for copy in o_swaps + [swap_far, swap]:
+        copy.wait_send()
+    for i, copy in enumerate((out_far, out_up, out_down)):
         copy.wait_recv()
         total = total + landed[i].astype(jnp.float32)
-    for copy in sends:
+    for copy in (out_far, out_up, out_down):
         copy.wait_send()
     out_ref[...] = total.astype(jnp.bfloat16)
 
@@ -350,7 +417,7 @@
     n_units = RING * RING
     return pl.pallas_call(
         kernel,
-        out_shape=jax.ShapeDtypeStruct(tokens.shape, bf16),
+        out_shape=pltpu.VMEM(tokens.shape, bf16),
         in_specs=[smem] + [hbm] * 8,
         out_specs=vmem,
         scratch_shapes=[
@@ -373,10 +440,10 @@
             pltpu.VMEM((BLOCK, 5 * HEAD_DIM), bf16),
             pltpu.VMEM((HALF, MODEL), bf16),
             pltpu.VMEM((HALF, MODEL), bf16),
-            pltpu.VMEM((HALF, MODEL), f32),
+            pltpu.VMEM((3 * ROWS, MODEL), bf16),
             pltpu.VMEM((3, ROWS, MODEL), bf16),
             dma((8,)), dma((8,)), dma((8,)), dma((n_units,)), dma((8,)), dma((64,)),
-            dma((2,)), dma((2,)), dma((4,)), dma((4,)),
+            dma((4,)), dma((4,)), dma((5,)), dma((5,)),
         ],
         compiler_params=pltpu.CompilerParams(
             collective_id=0, has_side_effects=True, vmem_limit_bytes=60 * 1024 * 1024),

time: 71.9 us -> 65.7 us (0.914)
  Pallas kernels: 69.5 us -> 64.3 us
  local copies, waits for them, and re-layouts: 1.47 us -> 0.63 us
    pallas_call x1, Pallas kernels: 69.5 us -> 64.3 us  [on_device(): pl.pallas_call(kernel, out_shape=pltpu.VMEM(tokens.shape, bf16), in_specs...]
    unnamed x1, local copies, waits for them, and re-layouts: 1.47 us -> 0.63 us
where the time goes in v3:
time: 65.7 us; the launch traced here: 65.6 us
  Pallas kernels  64.3 us (98%)
  between operations  0.66 us (1%)
    pallas_call x1, Pallas kernels, on_device(): pl.pallas_call(kernel, out_shape=pltpu.VMEM(tokens.shape, bf16), in_specs...  64.3 us

profile of v3, /device:TPU:1, one launch (start us, length us, event | category | flops | bytes accessed | tf_op | source)
XLA Modules:
  0.0 65.6 jit_solution(14369404906968943819)
XLA Ops:
  0.7 64.3 %shard_map.91 = bf16[32,1024]{1,0:T(8,128)(2,1)S(1)} custom-call(s32[1]{0:T(128)S(6)} %copy.12.valid_ref, bf16[32,1024]{1,0:T(8,128)(2,1)} %own_hbm.1, f32[1,1024]{1,0:T(1,128)} %bitcast.3, f32[1,128]{1,0:T(1,128)} %bitcast.4, f32[1,128]{1,0:T(1,128)} %bitcast.5, bf16[1024,512]{1,0:T(8,128)(2,1)} %w_query_hbm.1, bf16[1024,128]{1,0:T(8,128)(2,1)} %w_key_hbm.1, ...), custom_call_target="tpu_custom_call" | custom-call | tf_op jit(solution)/shard_map/pallas_call | solution.py:418
  65.0 0.6 copy.11

commit v4 on v3

--- a/solution.py
+++ b/solution.py
@@ -18,11 +18,12 @@
 MODEL = 1024
 
 LATE = 6
+EARLY = 1
 ORDER = [
-    (0, 0, 1, 1), (1, 1, 1, 2), (1, 0, 1, 0), (0, 0, 2, 0),
-    (2, 0, 1, 0), (1, 1, 2, 0), (1, 0, 2, 0), (0, 0, 3, 0),
-    (2, 0, 2, 0), (1, 1, 3, 0), (1, 0, 3, 0), (0, 0, 4, 0),
-    (2, 0, 3, 0), (1, 1, 4, 0), (1, 0, 4, 0), (2, 0, 4, 0),
+    (0, 0, 1, 1), (1, 1, 1, 0), (1, 0, 1, 0), (2, 0, 1, 0),
+    (0, 0, 2, 0), (1, 1, 2, 0), (1, 0, 2, 0), (2, 0, 2, 0),
+    (0, 0, 3, 0), (1, 1, 3, 0), (1, 0, 3, 0), (2, 0, 3, 0),
+    (0, 0, 4, 0), (1, 1, 4, 0), (1, 0, 4, 0), (2, 0, 4, 0),
 ]
 
 norm_eps = 1e-06
@@ -69,7 +70,7 @@
     def along(a_at, b_at):
         return {"sp": block_at(a_at, b_at), "tp": tp}
 
-    to_near = [along(2 * ((group + 1) % 4) + parity, b), along(2 * ((group + 3) % 4) + parity, b)]
+    to_near = [along(2 * ((group + ahead) % 4) + parity, b) for ahead in (1, 3, 2)]
     to_far = [along(a, (b + 1) % RING), along(a, (b + RING - 1) % RING)]
     to_pair = along(a + 1 - 2 * parity, b)
 
@@ -171,8 +172,8 @@
     def await_unit(unit):
         relay(unit, to_mate, near_send.at[0]).wait_recv()
 
-    def near_copy(way, d, side, unit):
-        return relay(unit, to_near[way], near_send.at[(way * 2 + d) * 2 + side])
+    def near_copy(way, side, unit):
+        return relay(unit, to_near[way], near_send.at[way * 2 + side])
 
     def far_copy(way, j, k, side, unit):
         return relay(unit, to_far[way], far_send.at[((way * 4 + j) * 4 + k) * 2 + side])
@@ -189,7 +190,8 @@
         units[unit, HALF:, :] = jnp.where(kept, values, 0.0).astype(jnp.bfloat16)
         for way in range(2):
             far_copy(way, 0, 0, side, unit).start()
-            near_copy(way, 0, side, unit).start()
+        for way in (0, 1, 2):
+            near_copy(way, side, unit).start()
         return normed
 
     def queries(normed, side):
@@ -227,8 +229,6 @@
             for way in range(2):
                 far_copy(way, chain(d, sign), 0, side, unit).start()
 
-            if d == 1 and sign == side:
-                near_copy(side, 1, side, unit).start()
 
     def attend(picks, heads):
         key = jnp.concatenate([units[u, :HALF, :] for u in picks], axis=1)
@@ -239,11 +239,15 @@
             return jnp.dot(q_scr[r], key, preferred_element_type=jnp.float32)
 
         heads = list(heads)
-        ahead = score(heads[0])
+        raw = score(heads[0])
+        ready = jnp.exp2(raw).astype(jnp.bfloat16)
+        raw = score(heads[1])
         for at, r in enumerate(heads):
-            weights = jnp.exp2(ahead).astype(jnp.bfloat16)
+            weights = ready
             if at + 1 < len(heads):
-                ahead = score(heads[at + 1])
+                ready = jnp.exp2(raw).astype(jnp.bfloat16)
+            if at + 2 < len(heads):
+                raw = score(heads[at + 2])
             acc[r] += jnp.dot(weights, both, preferred_element_type=jnp.float32)
 
     def lookup(i):
@@ -280,18 +284,10 @@
         def _():
             arrive(1, 1)
             arrive(1, 0)
-
-        @pl.when(step == 2)
-        def _():
             arrive(2, 0)
 
     def event(i, carry):
         exchange(i)
-
-        @pl.when(i == 0)
-        def _():
-            q_swap.wait_recv()
-
         attend(picks_of(i), range(8))
         return carry
 
@@ -300,7 +296,15 @@
         attend(picks_of(i), range(4, 8))
         return carry
 
-    lax.fori_loop(0, 16 - LATE, event, 0)
+    def early_event(i, carry):
+        exchange(i)
+        attend(picks_of(i), range(4))
+        return carry
+
+    lax.fori_loop(0, EARLY, early_event, 0)
+    q_swap.wait_recv()
+    attend([u for i in range(EARLY) for u in picks_of(i)], range(4, 8))
+    lax.fori_loop(EARLY, 16 - LATE, event, 0)
     lax.fori_loop(16 - LATE, 16, late_event, 0)
 
     small = lax.broadcasted_iota(jnp.int32, (BLOCK, HEAD_DIM), 1) // 32
@@ -326,14 +330,10 @@
             for way in range(2):
                 for k in range(4 if side == way else 3):
                     far_copy(way, j, k, side, unit).wait_send()
-
+            for way in range(3):
                 @pl.when(j == 0)
                 def _():
-                    near_copy(way, 0, side, unit).wait_send()
-
-            @pl.when(jnp.logical_and(d == 1, sign == side))
-            def _():
-                near_copy(side, 1, side, unit).wait_send()
+                    near_copy(way, side, unit).wait_send()
         return carry
 
     def catch_up(i, carry):
@@ -442,7 +442,7 @@
             pltpu.VMEM((HALF, MODEL), bf16),
             pltpu.VMEM((3 * ROWS, MODEL), bf16),
             pltpu.VMEM((3, ROWS, MODEL), bf16),
-            dma((8,)), dma((8,)), dma((8,)), dma((n_units,)), dma((8,)), dma((64,)),
+            dma((8,)), dma((8,)), dma((8,)), dma((n_units,)), dma((8,)), dma((72,)),
             dma((4,)), dma((4,)), dma((5,)), dma((5,)),
         ],
         compiler_params=pltpu.CompilerParams(

time: 65.7 us -> 65.3 us (level)
  no operation moved by 1% of the time
where the time goes in v4:
time: 65.3 us; the launch traced here: 65.2 us
  Pallas kernels  63.9 us (98%)
  between operations  0.66 us (1%)
    pallas_call x1, Pallas kernels, on_device(): pl.pallas_call(kernel, out_shape=pltpu.VMEM(tokens.shape, bf16), in_specs...  63.9 us

profile of v4, /device:TPU:1, one launch (start us, length us, event | category | flops | bytes accessed | tf_op | source)
XLA Modules:
  0.0 65.2 jit_solution(15534468977042613725)
XLA Ops:
  0.7 63.9 %shard_map.91 = bf16[32,1024]{1,0:T(8,128)(2,1)S(1)} custom-call(s32[1]{0:T(128)S(6)} %copy.12.valid_ref, bf16[32,1024]{1,0:T(8,128)(2,1)} %own_hbm.1, f32[1,1024]{1,0:T(1,128)} %bitcast.3, f32[1,128]{1,0:T(1,128)} %bitcast.4, f32[1,128]{1,0:T(1,128)} %bitcast.5, bf16[1024,512]{1,0:T(8,128)(2,1)} %w_query_hbm.1, bf16[1024,128]{1,0:T(8,128)(2,1)} %w_key_hbm.1, ...), custom_call_target="tpu_custom_call" | custom-call | tf_op jit(solution)/shard_map/pallas_call | solution.py:418
  64.5 0.6 copy.11

commit v5 on v4

--- a/solution.py
+++ b/solution.py
@@ -206,11 +206,11 @@
     first = project(0)
     tok_far.wait_recv()
     shares[2].start()
+    loads[6].wait()
+    queries(first, 0)
     for copy in shares:
         copy.wait_recv()
     other = project(1)
-    loads[6].wait()
-    queries(first, 0)
     queries(other, 1)
     q_swap = remote(q_scr.at[pl.ds(0, 4)], q_scr.at[pl.ds(4, 4)], pair_send.at[0],
                     pair_recv.at[0], to_pair)

time: 65.3 us -> 65.6 us (level)
  no operation moved by 1% of the time
where the time goes in v5:
time: 65.6 us; the launch traced here: 65.5 us
  Pallas kernels  64.2 us (98%)
  between operations  0.66 us (1%)
    pallas_call x1, Pallas kernels, on_device(): pl.pallas_call(kernel, out_shape=pltpu.VMEM(tokens.shape, bf16), in_specs...  64.2 us

profile of v5, /device:TPU:1, one launch (start us, length us, event | category | flops | bytes accessed | tf_op | source)
XLA Modules:
  0.0 65.5 jit_solution(9896204588082341927)
XLA Ops:
  0.7 64.2 %shard_map.91 = bf16[32,1024]{1,0:T(8,128)(2,1)S(1)} custom-call(s32[1]{0:T(128)S(6)} %copy.12.valid_ref, bf16[32,1024]{1,0:T(8,128)(2,1)} %own_hbm.1, f32[1,1024]{1,0:T(1,128)} %bitcast.3, f32[1,128]{1,0:T(1,128)} %bitcast.4, f32[1,128]{1,0:T(1,128)} %bitcast.5, bf16[1024,512]{1,0:T(8,128)(2,1)} %w_query_hbm.1, bf16[1024,128]{1,0:T(8,128)(2,1)} %w_key_hbm.1, ...), custom_call_target="tpu_custom_call" | custom-call | tf_op jit(solution)/shard_map/pallas_call | solution.py:418
  64.9 0.6 copy.11
